TPU v7x, 32 devices: a whole 2x2x4 slice. The times are simulated.
32 devices in a mesh: ep: 8 (over z, y), tp: 4 (over x, core).
Axes of the slice: x: 2, y: 2, z: 4, core: 2. Of those that a mesh axis runs over, the one named last changes fastest.
Arguments:
- queries: bfloat16 [4096, 2048], P('ep', 'tp'), may hold values from -6 to 6
- forget_pre: float32 [4096, 2048], P('ep', 'tp'), may hold values from -8 to 20
- value_in: bfloat16 [4096, 2048], P('ep', 'tp'), may hold values from -6 to 6
- out_gate: bfloat16 [4096, 2048], P('ep', 'tp'), may hold values from -6 to 6
- lower_bound: float32 [2048], P('tp'), may hold values from 0.5 to 0.8
- out_gain: float32 [128], replicated, may hold values from 0.1 to 1.9
- out_weight: bfloat16 [2048, 2048], P('tp'), may hold values from -0.125 to 0.125
- moe_tokens: bfloat16 [2048, 2048], P('ep'), may hold values from -6 to 6
- moe_gain: float32 [2048], replicated, may hold values from 0.1 to 1.9
- expert_ids: int32 [2048, 4], P('ep'), may hold values from 0 to 15, all different within a row; in each aligned block of 64 rows (0 to 63, 64 to 127, ...) at most 32 rows name the same one
- route_weights: float32 [2048, 4], P('ep'), may hold values from 0.1 to 1
- w_gate: bfloat16 [16, 2048, 1024], P('ep', None, 'tp'), may hold values from -0.125 to 0.125
- w_up: bfloat16 [16, 2048, 1024], P('ep', None, 'tp'), may hold values from -0.125 to 0.125
- w_down: bfloat16 [16, 1024, 2048], P('ep', 'tp'), may hold values from -0.1875 to 0.1875
Outputs:
- mixer_out: bfloat16 [4096, 2048], P(('ep', 'tp'))
- expert_out: bfloat16 [2048, 2048], P(('ep', 'tp'))
Inputs may be any that keep to these rules, and one draw needn't show every extreme that they name: `expert_ids`: each row names 4 different experts. In each aligned block of 64 rows no expert is named by more than 32 rows, and in some block some expert is named by exactly 32 rows.
All inputs are finite; a program needn't handle non-finite values.
Results may differ from a plain program's by a relative error of at most 0.01065.
Values may be sent and summed in bfloat16 or wider, within the bound.
A program may use at most 128 MiB of HBM per device.

v0:
```python
import jax
import jax.numpy as jnp
from jax import lax
from jax.sharding import PartitionSpec as P

HEAD_DIM = 128
BLOCK = 64
EPS = 1e-06
HIGHEST = lax.Precision.HIGHEST


def prefix(part, axis, combine, identity):
    place = lax.axis_index(axis)
    gathered = jax.tree.map(lambda a: lax.all_gather(a, axis), part)
    state = jax.tree.map(lambda a, e: jnp.zeros_like(a) + jnp.asarray(e, a.dtype), part, identity)

    def one(hop, state):
        return combine(
            state, jax.tree.map(lambda a: lax.dynamic_index_in_dim(a, hop, 0, False), gathered)
        )

    return lax.fori_loop(0, place, one, state)


def rms_scale(values, gain):
    return values * lax.rsqrt(jnp.mean(values * values, axis=-1, keepdims=True) + EPS) * gain


def block_step(memory, inputs):
    queries_block, weight_block, values_block, forget_block = inputs
    cumulative = jnp.cumsum(forget_block, axis=1)
    length = queries_block.shape[1]
    causal = (
        jnp.arange(length, dtype=jnp.int32)[:, None] >= jnp.arange(length, dtype=jnp.int32)[None, :]
    )
    decayed_query = queries_block * jnp.exp(cumulative)
    decayed_key = weight_block * jnp.exp(-cumulative)
    carried_out = jnp.einsum("htd,hde->hte", decayed_query, memory, precision=HIGHEST)
    scores = jnp.einsum("htd,hsd->hts", decayed_query, decayed_key, precision=HIGHEST)
    scores = jnp.where(causal[None], scores, 0.0)
    local_out = jnp.einsum("hts,hse->hte", scores, values_block, precision=HIGHEST)
    block_total = cumulative[:, -1:, :]
    added = jnp.einsum(
        "hsd,hse->hde",
        weight_block * jnp.exp(block_total - cumulative),
        values_block,
        precision=HIGHEST,
    )
    memory = jnp.exp(block_total[:, 0, :])[:, :, None] * memory + added
    return (memory, carried_out + local_out)


def to_blocks(array, head_count):
    row_count = array.shape[0]
    return (
        array.astype(jnp.float32)
        .reshape(row_count // BLOCK, BLOCK, head_count, HEAD_DIM)
        .transpose(0, 2, 1, 3)
    )


def combine_memory(earlier, later):
    return (earlier[0] * later[0], later[0][:, :, None] * earlier[1] + later[1])


def slot_ranks(ids_block, expert_count):
    onehot = (
        ids_block[:, :, None] == jnp.arange(expert_count, dtype=jnp.int32)[None, None, :]
    ).astype(jnp.int32)
    return jnp.sum(onehot * (jnp.cumsum(onehot, axis=1) - 1), axis=2)


def local(
    queries,
    forget_pre,
    value_in,
    out_gate,
    lower_bound,
    out_gain,
    out_weight,
    moe_tokens,
    moe_gain,
    expert_ids,
    route_weights,
    w_gate,
    w_up,
    w_down,
):
    lanes = lax.axis_size("tp")
    lane_index = lax.axis_index("tp")
    ep_count = lax.axis_size("ep")
    seq_rows, local_width = queries.shape
    model_width = out_weight.shape[1]
    head_count = local_width // HEAD_DIM
    weight_in = (1.0 - lower_bound) * jax.nn.sigmoid(-forget_pre)
    log_forget = jnp.log1p(-weight_in)
    cumulative = jnp.cumsum(log_forget, axis=0)
    span_total = cumulative[-1]
    to_end = (weight_in * jnp.exp(span_total[None, :] - cumulative)).reshape(
        seq_rows, head_count, HEAD_DIM
    )
    values_float = value_in.astype(jnp.float32).reshape(seq_rows, head_count, HEAD_DIM)
    local_memory = jnp.einsum("shd,she->hde", to_end, values_float, precision=HIGHEST)
    decay_total = jnp.exp(span_total).reshape(head_count, HEAD_DIM)
    neutral = (jnp.ones_like(decay_total), jnp.zeros_like(local_memory))
    earlier_part = prefix((decay_total, local_memory), "ep", combine_memory, neutral)
    final_memory, outputs = lax.scan(
        block_step,
        earlier_part[1],
        (
            to_blocks(queries, head_count),
            to_blocks(weight_in, head_count),
            to_blocks(value_in, head_count),
            to_blocks(log_forget, head_count),
        ),
    )
    outputs = outputs.transpose(0, 2, 1, 3).reshape(seq_rows, head_count, HEAD_DIM)
    gate_act = jax.nn.silu(out_gate.astype(jnp.float32)).reshape(seq_rows, head_count, HEAD_DIM)
    gated = (
        (rms_scale(outputs, out_gain) * gate_act)
        .reshape(seq_rows, local_width)
        .astype(jnp.bfloat16)
    )
    qrows = moe_tokens.shape[0] // lanes
    top_count = expert_ids.shape[1]
    local_experts = w_gate.shape[0]
    expert_count = local_experts * ep_count
    capacity = max(2, 2 * qrows * top_count // expert_count)
    send_tokens = lax.dynamic_slice_in_dim(moe_tokens, lane_index * qrows, qrows, 0)
    send_ids = lax.dynamic_slice_in_dim(expert_ids, lane_index * qrows, qrows, 0)
    quarters = send_tokens.shape[0] // qrows
    normed = rms_scale(send_tokens.astype(jnp.float32), moe_gain).astype(jnp.bfloat16)
    ids_block = send_ids.reshape(quarters, qrows * top_count)
    ranks = slot_ranks(ids_block, expert_count)
    quarter_base = jnp.arange(quarters, dtype=jnp.int32)[:, None] * (expert_count * capacity)
    slot_index = (quarter_base + ids_block * capacity + ranks).reshape(-1)
    source_row = jnp.arange(quarters * qrows * top_count, dtype=jnp.int32) // top_count
    sources = (
        jnp.full((quarters * expert_count * capacity,), quarters * qrows, jnp.int32)
        .at[slot_index]
        .set(source_row)
    )
    padded = jnp.concatenate([normed, jnp.zeros((1, model_width), jnp.bfloat16)], axis=0)
    outgoing = padded[sources].reshape(quarters, ep_count, local_experts * capacity, model_width)
    arrived = lax.all_to_all(outgoing, "ep", split_axis=1, concat_axis=1, tiled=True)
    piece = lax.all_gather(arrived, "tp", axis=0, tiled=True)
    shaped = piece.reshape(piece.shape[0], ep_count, local_experts, capacity, model_width)
    gate_pre = jnp.einsum("qsecd,edf->qsecf", shaped, w_gate, preferred_element_type=jnp.float32)
    up_pre = jnp.einsum("qsecd,edf->qsecf", shaped, w_up, preferred_element_type=jnp.float32)
    hidden = (jax.nn.silu(gate_pre) * up_pre).astype(jnp.bfloat16)
    lane_rows = ep_count * local_experts * capacity
    mixer_sum = lax.psum_scatter(
        jnp.dot(gated, out_weight, preferred_element_type=jnp.float32).astype(jnp.bfloat16),
        "tp",
        scatter_dimension=0,
        tiled=True,
    )
    projected = jnp.einsum("qsecf,efd->qsecd", hidden, w_down, preferred_element_type=jnp.float32)
    expert_sum = lax.psum_scatter(
        projected.reshape(lax.axis_size("tp") * lane_rows, model_width).astype(jnp.bfloat16),
        "tp",
        scatter_dimension=0,
        tiled=True,
    )
    leaving = expert_sum.reshape(ep_count, local_experts * capacity, model_width)
    returned = lax.all_to_all(leaving, "ep", split_axis=0, concat_axis=0, tiled=True)
    returned = returned.reshape(expert_count * capacity, model_width)
    own_quarter = lane_index * (quarters // lanes)
    own_ids = lax.dynamic_index_in_dim(ids_block, own_quarter, 0, keepdims=False)
    own_ranks = lax.dynamic_index_in_dim(ranks, own_quarter, 0, keepdims=False)
    picked = (
        returned[own_ids * capacity + own_ranks]
        .astype(jnp.float32)
        .reshape(qrows, top_count, model_width)
    )
    own_weights = lax.dynamic_slice_in_dim(route_weights, lane_index * qrows, qrows, 0)
    expert_out = jnp.sum(picked * own_weights[:, :, None], axis=1).astype(jnp.bfloat16)
    return (mixer_sum, expert_out)


def solution(mesh):
    in_specs = (
        P("ep", "tp"),
        P("ep", "tp"),
        P("ep", "tp"),
        P("ep", "tp"),
        P("tp"),
        P(),
        P("tp", None),
        P("ep", None),
        P(),
        P("ep", None),
        P("ep", None),
        P("ep", None, "tp"),
        P("ep", None, "tp"),
        P("ep", "tp", None),
    )
    out_specs = (P(("ep", "tp"), None), P(("ep", "tp"), None))
    return jax.shard_map(local, mesh=mesh, in_specs=in_specs, out_specs=out_specs, check_vma=False)
```

profile of v0, /device:TPU:0, one launch (start us, length us, event | category | flops | bytes accessed | tf_op | source)
XLA Modules:
  0.0 324.8 jit_solution(6466362243241929309)
XLA Ops:
  9.6 1.4 scatter_custom_fusion
  13.3 3.3 %gather_fusion = bf16[512,2048]{1,0:T(8,128)(2,1)} fusion(bf16[65,2048]{1,0:T(8,128)(2,1)S(1)} %concatenate.3, s32[1024]{0:T(1024)S(1)} %pad_clamp_fusion.1), kind=kCustom, calls=%fused_computation | custom fusion | bytes 4196352 | tf_op jit(solution)/shard_map/gather | solution.py:144
  16.7 55.6 %all_to_all.10 = bf16[1,8,64,2048]{3,2,0,1:T(8,128)(2,1)} all-to-all(bf16[1,8,64,2048]{3,2,0,1:T(8,128)(2,1)} %bitcast.171), channel_id=1, replica_groups=mesh['ep'=8,'tp'=4] {'ep'}, dimensions={1} | all-to-all | bytes 4194304 | tf_op jit(solution)/shard_map/all_to_all | solution.py:145
  73.0 2.8 negate_log-plus-one_fusion
  77.5 1.5 broadcast_add_fusion
  80.6 2.6 copy.104
  83.3 2.8 fusion.40
  86.3 43.4 %all-gather.4.cloned.1.call-done = bf16[4,8,64,2048]{3,2,1,0:T(8,128)(2,1)} async-done(((bf16[1,8,64,2048]{3,2,1,0:T(8,128)(2,1)}), bf16[4,8,64,2048]{3,2,1,0:T(8,128)(2,1)}) %all-gather.4.cloned.1.call-update) | async-done | bytes 8388624 | tf_op jit(solution)/shard_map/all_gather | solution.py:146
  129.8 6.5 %fusion.15 = f32[2,4,8,32,256]{4,3,2,1,0:T(8,128)S(1)} fusion(bf16[4,8,2,32,2048]{4,3,2,1,0:T(8,128)(2,1)} %bitcast.199, bf16[2,2048,256]{2,1,0:T(8,128)(2,1)} %param.29), kind=kOutput, calls=%fused_computation.31 | convolution fusion | flops 2147483648 | bytes 12582912 | tf_op jit(solution)/shard_map/qsecd,edf->qsecf/dot_general | solution.py:148
  136.7 2.6 fusion.20
  139.4 5.6 %convert_bitcast_fusion = bf16[4,8,2,32,2048]{4,3,1,0,2:T(8,128)(2,1)} fusion(bf16[4,8,2,32,256]{4,3,1,0,2:T(8,128)(2,1)S(1)} %fusion.20, bf16[2,256,2048]{2,1,0:T(8,128)(2,1)S(1)} %copy-done), kind=kOutput, calls=%fused_computation.28 | convolution fusion | flops 2151677952 | bytes 11534336 | tf_op jit(solution)/shard_map/qsecf,efd->qsecd/dot_general | solution.py:158
  144.9 8.3 %copy.99 = bf16[4,8,2,32,2048]{4,3,2,1,0:T(8,128)(2,1)} copy(bf16[4,8,2,32,2048]{4,3,1,0,2:T(8,128)(2,1)} %convert_bitcast_fusion) | data formatting | bytes 16777216 | tf_op jit(solution)/shard_map/convert_element_type | solution.py:160
  153.3 1.3 reshape.281
  155.1 1.3 reshape.297
  156.4 2.4 reshape.298
  158.8 26.6 %all_gather.12 = f32[8,4,128]{2,1,0:T(4,128)S(1)} all-gather(f32[1,4,128]{2,1,0:T(4,128)S(1)} %bitcast.193), channel_id=1, replica_groups=mesh['ep'=8,'tp'=4] {'ep'}, dimensions={0}, use_global_device_ids=true | all-gather | bytes 18432 | tf_op jit(solution)/shard_map/all_gather | solution.py:14
  185.7 30.8 %while.25 = (s32[]{:T(128)}, f32[4,128,128]{2,1,0:T(8,128)S(1)}, f32[8,4,64,128]{3,2,1,0:T(8,128)S(1)}, f32[8,4,64,128]{3,1,2,0:T(4,128)}, f32[8,4,64,128]{3,1,2...) while((s32[]{:T(128)}, f32[4,128,128]{2,1,0:T(8,128)S(1)}, ...), condition=%wide.region_6.7_spmd, body=%wide.region_4.6_spmd.sunk | while | flops 153440256 | bytes 4083821 | solution.py:107
  218.4 4.3 %convolution_convert_fusion = bf16[512,2048]{1,0:T(8,128)(2,1)} fusion(bf16[512,2048]{1,0:T(8,128)(2,1)} %param.24, bf16[512,512]{1,0:T(8,128)(2,1)S(1)} %copy-done.11, f32[64,8,4,128]{3,2,1,0:T(4,128)S(1)} %bitcast.183, f32[64,8,4,128]{3,2,1,0:T(4,128)S(1)} %bitcast.185, f32[512]{0:T(512)S(1)} %broadcast_bitcast_fusion), kind=kOutput, calls=%fused_computation.33 | convolution fusion | flops 1077149696 | bytes 6817792 | tf_op jit(solution)/shard_map/dot_general | solution.py:153
  222.7 31.7 %reduce-scatter.5.cloned.1.call-done = bf16[512,2048]{1,0:T(8,128)(2,1)} async-done(((bf16[2048,2048]{1,0:T(8,128)(2,1)}), bf16[512,2048]{1,0:T(8,128)(2,1)}) %reduce-scatter.5.cloned.1.call-update) | async-done | bytes 2097168 | tf_op jit(solution)/shard_map/reduce_scatter | solution.py:159
  254.4 5.7 %all-to-all-start.1 = ((bf16[8,64,2048]{2,1,0:T(8,128)(2,1)}), bf16[8,64,2048]{2,1,0:T(8,128)(2,1)}, u32[]{:S(2)}, u32[]{:S(2)}) async-start(bf16[8,64,2048]{2,1,0:T(8,128)(2,1)} %bitcast.182), calls=%async_computation.3 | async-start | bytes 4194304 | tf_op jit(solution)/shard_map/all_to_all | solution.py:166
  260.2 48.0 %all-to-all-done.1 = bf16[8,64,2048]{2,1,0:T(8,128)(2,1)} async-done(((bf16[8,64,2048]{2,1,0:T(8,128)(2,1)}), bf16[8,64,2048]{2,1,0:T(8,128)(2,1)}, u32[]{:S(2)}, u32[]{:S(2)}) %all-to-all-start.1) | async-done | bytes 2097184 | tf_op jit(solution)/shard_map/all_to_all | solution.py:166
  308.2 4.4 %gather_fusion.1 = bf16[256,2048]{1,0:T(8,128)(2,1)S(1)} fusion(bf16[512,2048]{1,0:T(8,128)(2,1)} %bitcast.48, s32[1024]{0:T(1024)S(1)} %pad_clamp_fusion), kind=kCustom, calls=%fused_computation.1 | custom fusion | bytes 2098176 | tf_op jit(solution)/shard_map/gather | solution.py:172
  312.6 1.7 reshape.296
  314.3 3.9 %multiply_reduce_fusion = bf16[64,2048]{1,0:T(8,128)(2,1)} fusion(f32[64,4,2048]{2,1,0:T(4,128)} %reshape.296, f32[64,4]{1,0:T(8,128)S(1)} %copy.100), kind=kLoop, calls=%fused_computation.44 | loop fusion | flops 917504 | bytes 2360320 | tf_op jit(solution)/shard_map/reduce_sum | solution.py:177
  (167 shorter events, 42.2 us)
Async XLA Ops:
  7.2 132.2 %copy-start = (bf16[2,256,2048]{2,1,0:T(8,128)(2,1)S(1)}, bf16[2,256,2048]{2,1,0:T(8,128)(2,1)}, u32[]{:S(2)}) copy-start(bf16[2,256,2048]{2,1,0:T(8,128)(2,1)} %param.31) | copy-start | bytes 6291460
  7.2 122.6 %all-gather.4.cloned.1.call-start = ((), (), s32[]{:S(2)}) async-start(), calls=%async_computation.5 | async-start | bytes 10485760 | tf_op jit(solution)/shard_map/all_gather | solution.py:146
  72.3 0.7 copy-start.6
  72.4 113.1 %all-gather.6.cloned.1.call-start = ((), (), s32[]{:S(2)}) async-start(), calls=%async_computation.7 | async-start | bytes 2359296 | tf_op jit(solution)/shard_map/all_gather | solution.py:14
  76.5 1.0 copy-start.4
  77.5 1.9 copy-start.2
  86.1 168.3 %reduce-scatter.5.cloned.1.call-start = ((), (), s32[]{:S(2)}) async-start(), calls=%async_computation.6 | async-start | bytes 10485760 | tf_op jit(solution)/shard_map/reduce_scatter | solution.py:159
  129.8 6.5 %copy-start.9 = (bf16[4,8,64,2048]{3,2,1,0:T(8,128)(2,1)S(1)}, bf16[4,8,64,2048]{3,2,1,0:T(8,128)(2,1)}, u32[]{:S(2)}) copy-start(bf16[4,8,64,2048]{3,2,1,0:T(8,128)(2,1)} %all-gather.4.cloned.1.call-done) | copy-start | bytes 25165828
  129.8 7.0 %copy-start.10 = (bf16[2,2048,256]{2,1,0:T(8,128)(2,1)S(1)}, bf16[2,2048,256]{2,1,0:T(8,128)(2,1)}, u32[]{:S(2)}) copy-start(bf16[2,2048,256]{2,1,0:T(8,128)(2,1)} %param.30) | copy-start | bytes 6291460
  153.3 1.4 copy-start.3
  153.3 164.9 %reduce-scatter.3.cloned.1.call-start = ((), (), s32[]{:S(2)}) async-start(), calls=%async_computation.4 | async-start | bytes 2621440 | tf_op jit(solution)/shard_map/reduce_scatter | solution.py:152
  153.3 1.7 copy-start.5
  155.0 30.4 %copy-start.8 = (f32[128]{0:T(128)S(1)}, f32[128]{0:T(128)}, u32[]{:S(2)}) copy-start(f32[128]{0:T(128)} %param.23) | copy-start | bytes 1540
  216.9 1.5 copy-start.11
  254.4 5.7 %copy-start.7 = (f32[256,4]{0,1:T(4,128)S(1)}, f32[256,4]{0,1:T(4,128)}, u32[]{:S(2)}) copy-start(f32[256,4]{0,1:T(4,128)} %param.28) | copy-start | bytes 12292
  254.4 53.8 %all-to-all-start.1 = ((bf16[8,64,2048]{2,1,0:T(8,128)(2,1)}), bf16[8,64,2048]{2,1,0:T(8,128)(2,1)}, u32[]{:S(2)}, u32[]{:S(2)}) async-start(bf16[8,64,2048]{2,1,0:T(8,128)(2,1)} %bitcast.182), calls=%async_computation.3 | async-start | bytes 4194304 | tf_op jit(solution)/shard_map/all_to_all | solution.py:166
  308.2 10.0 %copy-start.1 = (bf16[2,256,2048]{2,1,0:T(8,128)(2,1)S(1)}, bf16[2,256,2048]{2,1,0:T(8,128)(2,1)}, u32[]{:S(2)}) copy-start(bf16[2,256,2048]{2,1,0:T(8,128)(2,1)} %param.31) | copy-start | bytes 6291460
Sparse Core Ops, SparseCore 0:
  72.5 57.2 all-gather.3
  132.5 49.1 all-gather.5
  184.3 70.0 reduce-scatter.4
  257.3 31.1 reduce-scatter.2
where the time goes:
time: 326 us; the launch traced here: 325 us
  waiting for transfers between devices  123 us (38%)
  blocking collectives  82.3 us (25%)
  local copies, waits for them, and re-layouts  47.9 us (15%)
  matrix products  34.9 us (11%)
  other arithmetic  15.5 us (5%)
  between operations  14.1 us (4%)
  starting transfers between devices  6 us (2%)
    all_to_all x1, blocking collectives, local(): lax.all_to_all(outgoing, 'ep', split_axis=1, concat_axis=1, tiled=True)  55.6 us
    all_to_all x1, waiting for transfers between devices, local(): lax.all_to_all(leaving, 'ep', split_axis=0, concat_axis=0, tiled=True)  48 us
    all_gather x1, waiting for transfers between devices, local(): piece = lax.all_gather(arrived, 'tp', axis=0, tiled=True)  43.4 us
    reduce_scatter x1, waiting for transfers between devices, local(): lax.psum_scatter(projected.reshape(lax.axis_size('tp') * lane_rows, model...  31.7 us
    all_gather x1, blocking collectives, prefix(): gathered = jax.tree.map(lambda a: lax.all_gather(a, axis), part)  26.6 us
    dynamic_slice x24, local copies, waits for them, and re-layouts, local(): lax.scan(block_step, earlier_part[1], (to_blocks(queries, head_count), to...  15.7 us
    convert_element_type x1, local copies, waits for them, and re-layouts, local(): projected.reshape(lax.axis_size('tp') * lane_rows, model_width)  8.31 us
  transfers between devices with their start and end apart: 5, of which 3 were waited for; matrix products, arithmetic and copies ran while one was open for 27% of the time, Pallas kernels for 0%

commit v1 on v0

--- a/solution.py
+++ b/solution.py
@@ -1,3 +1,4 @@
+import functools
 import jax
 import jax.numpy as jnp
 from jax import lax
@@ -7,6 +8,23 @@
 BLOCK = 64
 EPS = 1e-06
 HIGHEST = lax.Precision.HIGHEST
+
+
+def node_plan(matrix, which_dim):
+    chips = lax.axis_size("tp")
+    local_part = sorted(((dev_i, (dev_i + 1) % chips) for dev_i in range(chips)))
+    plain = matrix
+    heap = [plain]
+    for src_i in tuple(range(1, chips)):
+        plain = lax.ppermute(plain, axis_name="tp", perm=local_part)
+        heap.insert(0, plain)
+    last = jnp.concatenate(heap, which_dim)
+    y2 = lax.axis_index("tp")
+    w2 = jnp.roll(last, (y2 + 1) * matrix.shape[which_dim], which_dim)
+    return w2
+
+
+_form_meshes = functools.partial(node_plan, which_dim=0)
 
 
 def prefix(part, axis, combine, identity):
@@ -143,7 +161,7 @@
     padded = jnp.concatenate([normed, jnp.zeros((1, model_width), jnp.bfloat16)], axis=0)
     outgoing = padded[sources].reshape(quarters, ep_count, local_experts * capacity, model_width)
     arrived = lax.all_to_all(outgoing, "ep", split_axis=1, concat_axis=1, tiled=True)
-    piece = lax.all_gather(arrived, "tp", axis=0, tiled=True)
+    piece = _form_meshes(arrived)
     shaped = piece.reshape(piece.shape[0], ep_count, local_experts, capacity, model_width)
     gate_pre = jnp.einsum("qsecd,edf->qsecf", shaped, w_gate, preferred_element_type=jnp.float32)
     up_pre = jnp.einsum("qsecd,edf->qsecf", shaped, w_up, preferred_element_type=jnp.float32)

time: 326 us -> 352 us (1.080)
  local copies, waits for them, and re-layouts: 47.9 us -> 79.6 us
  waiting for transfers between devices: 123 us -> 108 us
  starting transfers between devices: 6 us -> 10.9 us
    ppermute x0 -> x3, waiting for transfers between devices: none -> 64.9 us  [node_plan(): plain = lax.ppermute(plain, axis_name='tp', perm=local_part)]
    all_gather x1 -> x0, waiting for transfers between devices: 43.4 us -> none  [local(): piece = lax.all_gather(arrived, 'tp', axis=0, tiled=True)]
    reduce_scatter x1, waiting for transfers between devices: 31.7 us -> 0.03 us  [local(): lax.psum_scatter(projected.reshape(lax.axis_size('tp') * lane_rows, model...]
    unnamed x25 -> x46, local copies, waits for them, and re-layouts: 2.12 us -> 22.7 us
    dynamic_slice x0 -> x1, local copies, waits for them, and re-layouts: none -> 8.44 us  [node_plan(): w2 = jnp.roll(last, (y2 + 1) * matrix.shape[which_dim], which_dim)]
    dot_general x8, matrix products: 2.95 us -> 8.23 us  [block_step(): jnp.einsum('htd,hde->hte', decayed_query, memory, precision=HIGHEST)]
    all_to_all x1, starting transfers between devices: 5.66 us -> 10.6 us  [local(): lax.all_to_all(leaving, 'ep', split_axis=0, concat_axis=0, tiled=True)]
    all_to_all x1, waiting for transfers between devices: 48 us -> 43.3 us  [local(): lax.all_to_all(leaving, 'ep', split_axis=0, concat_axis=0, tiled=True)]
  transfers between devices with their start and end apart: 5 -> 7, of which waited for: 3 -> 4; matrix products, arithmetic and copies ran while one was open for 27% -> 34% of each run, Pallas kernels for 0% -> 0%
where the time goes in v1:
time: 352 us; the launch traced here: 351 us
  waiting for transfers between devices  108 us (31%)
  blocking collectives  81.8 us (23%)
  local copies, waits for them, and re-layouts  79.6 us (23%)
  matrix products  37.9 us (11%)
  between operations  15.8 us (4%)
  other arithmetic  15.5 us (4%)
  starting transfers between devices  10.9 us (3%)
    ppermute x3, waiting for transfers between devices, node_plan(): plain = lax.ppermute(plain, axis_name='tp', perm=local_part)  64.9 us
    all_to_all x1, blocking collectives, local(): lax.all_to_all(outgoing, 'ep', split_axis=1, concat_axis=1, tiled=True)  55.7 us
    all_to_all x1, waiting for transfers between devices, local(): lax.all_to_all(leaving, 'ep', split_axis=0, concat_axis=0, tiled=True)  43.3 us
    all_gather x1, blocking collectives, prefix(): gathered = jax.tree.map(lambda a: lax.all_gather(a, axis), part)  26.1 us
    unnamed x46, local copies, waits for them, and re-layouts  22.7 us
    dynamic_slice x24, local copies, waits for them, and re-layouts, local(): lax.scan(block_step, earlier_part[1], (to_blocks(queries, head_count), to...  16 us
    all_to_all x1, starting transfers between devices, local(): lax.all_to_all(leaving, 'ep', split_axis=0, concat_axis=0, tiled=True)  10.6 us
    dynamic_slice x1, local copies, waits for them, and re-layouts, node_plan(): w2 = jnp.roll(last, (y2 + 1) * matrix.shape[which_dim], which_dim)  8.44 us
  transfers between devices with their start and end apart: 7, of which 4 were waited for; matrix products, arithmetic and copies ran while one was open for 34% of the time, Pallas kernels for 0%

profile of v1, /device:TPU:0, one launch (start us, length us, event | category | flops | bytes accessed | tf_op | source)
XLA Modules:
  0.0 350.5 jit_solution(16510293347616376082)
XLA Ops:
  14.2 3.3 gather_fusion
  17.5 55.7 %all_to_all.10 = bf16[1,8,64,2048]{3,2,0,1:T(8,128)(2,1)S(1)} all-to-all(bf16[1,8,64,2048]{3,2,0,1:T(8,128)(2,1)} %bitcast.178), channel_id=1, replica_groups=mesh['ep'=8,'tp'=4] {'ep'}, dimensions={1} | all-to-all | bytes 4194304 | tf_op jit(solution)/shard_map/all_to_all | solution.py:163
  74.5 25.5 %collective-permute-done = bf16[1,8,64,2048]{3,2,1,0:T(8,128)(2,1)S(1)} collective-permute-done((bf16[1,8,64,2048]{3,2,1,0:T(8,128)(2,1)S(1)}, bf16[1,8,64,2048]{3,2,1,0:T(8,128)(2,1)S(1)}, u32[]{:S(2)}, u32[]{:S(2)}) %collective-permute-start) | collective-permute-done | bytes 2097184 | tf_op jit(solution)/shard_map/ppermute | solution.py:19
  101.3 25.6 %collective-permute-done.1 = bf16[1,8,64,2048]{3,2,1,0:T(8,128)(2,1)} collective-permute-done((bf16[1,8,64,2048]{3,2,1,0:T(8,128)(2,1)S(1)}, bf16[1,8,64,2048]{3,2,1,0:T(8,128)(2,1)}, u32[]{:S(2)}, u32[]{:S(2)}) %collective-permute-start.1) | collective-permute-done | bytes 2097184 | tf_op jit(solution)/shard_map/ppermute | solution.py:19
  133.3 2.5 copy.110
  135.8 2.7 fusion.40
  138.8 13.9 %collective-permute-done.2 = bf16[1,8,64,2048]{3,2,1,0:T(8,128)(2,1)} collective-permute-done((bf16[1,8,64,2048]{3,2,1,0:T(8,128)(2,1)}, bf16[1,8,64,2048]{3,2,1,0:T(8,128)(2,1)}, u32[]{:S(2)}, u32[]{:S(2)}) %collective-permute-start.2) | collective-permute-done | bytes 2097184 | tf_op jit(solution)/shard_map/ppermute | solution.py:19
  152.6 3.2 constant_dynamic-update-slice_fusion.7
  155.8 3.3 constant_dynamic-update-slice_fusion.6
  163.0 3.2 constant_dynamic-update-slice_fusion.3
  166.2 3.1 constant_dynamic-update-slice_fusion.2
  172.2 8.4 %constant_dynamic-slice_fusion.5 = bf16[4,8,64,2048]{3,2,1,0:T(8,128)(2,1)} fusion(bf16[8,8,64,2048]{3,2,1,0:T(8,128)(2,1)} %constant_dynamic-update-slice_fusion, s32[]{:T(128)S(6)} %select_n.57), kind=kLoop, calls=%fused_computation.102 | loop fusion | bytes 16777220 | tf_op jit(solution)/shard_map/jit(_roll_dynamic)/dynamic_slice | solution.py:23
  180.7 5.9 %fusion.15 = f32[2,4,8,32,256]{4,3,2,1,0:T(8,128)S(1)} fusion(bf16[4,8,2,32,2048]{4,3,2,1,0:T(8,128)(2,1)} %bitcast.176, bf16[2,2048,256]{2,1,0:T(8,128)(2,1)S(1)} %copy-done.15), kind=kOutput, calls=%fused_computation.31 | convolution fusion | flops 2147483648 | bytes 12582912 | tf_op jit(solution)/shard_map/qsecd,edf->qsecf/dot_general | solution.py:166
  187.0 2.6 fusion.20
  189.7 5.6 %convert_bitcast_fusion = bf16[4,8,2,32,2048]{4,3,1,0,2:T(8,128)(2,1)} fusion(bf16[4,8,2,32,256]{4,3,1,0,2:T(8,128)(2,1)S(1)} %fusion.20, bf16[2,256,2048]{2,1,0:T(8,128)(2,1)S(1)} %copy-done), kind=kOutput, calls=%fused_computation.28 | convolution fusion | flops 2151677952 | bytes 11534336 | tf_op jit(solution)/shard_map/qsecf,efd->qsecd/dot_general | solution.py:176
  195.3 8.3 %copy.105 = bf16[4,8,2,32,2048]{4,3,2,1,0:T(8,128)(2,1)} copy(bf16[4,8,2,32,2048]{4,3,1,0,2:T(8,128)(2,1)} %convert_bitcast_fusion) | data formatting | bytes 16777216 | tf_op jit(solution)/shard_map/convert_element_type | solution.py:178
  204.9 2.6 reshape.282
  210.2 26.1 %all_gather.9 = f32[8,4,128]{2,1,0:T(4,128)S(1)} all-gather(f32[1,4,128]{2,1,0:T(4,128)S(1)} %bitcast.197), channel_id=1, replica_groups=mesh['ep'=8,'tp'=4] {'ep'}, dimensions={0}, use_global_device_ids=true | all-gather | bytes 18432 | tf_op jit(solution)/shard_map/all_gather | solution.py:32
  236.6 36.3 %while.25 = (s32[]{:T(128)}, f32[4,128,128]{2,1,0:T(8,128)S(1)}, f32[8,4,64,128]{3,2,1,0:T(8,128)}, f32[8,4,64,128]{3,1,2,0:T(4,128)}, f32[8,4,64,128]{3,1,2,0:T...) while((s32[]{:T(128)}, f32[4,128,128]{2,1,0:T(8,128)S(1)}, ...), condition=%wide.region_6.7_spmd, body=%wide.region_4.6_spmd.sunk | while | flops 153440256 | bytes 4084329 | solution.py:125
  276.4 2.7 convolution_convert_fusion
  279.2 10.6 %all-to-all-start.1 = ((bf16[8,64,2048]{2,1,0:T(8,128)(2,1)}), bf16[8,64,2048]{2,1,0:T(8,128)(2,1)}, u32[]{:S(2)}, u32[]{:S(2)}) async-start(bf16[8,64,2048]{2,1,0:T(8,128)(2,1)} %bitcast.186), calls=%async_computation.3 | async-start | bytes 4194304 | tf_op jit(solution)/shard_map/all_to_all | solution.py:184
  289.9 43.3 %all-to-all-done.1 = bf16[8,64,2048]{2,1,0:T(8,128)(2,1)} async-done(((bf16[8,64,2048]{2,1,0:T(8,128)(2,1)}), bf16[8,64,2048]{2,1,0:T(8,128)(2,1)}, u32[]{:S(2)}, u32[]{:S(2)}) %all-to-all-start.1) | async-done | bytes 2097184 | tf_op jit(solution)/shard_map/all_to_all | solution.py:184
  333.3 4.2 %gather_fusion.1 = bf16[256,2048]{1,0:T(8,128)(2,1)S(1)} fusion(bf16[512,2048]{1,0:T(8,128)(2,1)} %bitcast.50, s32[1024]{0:T(1024)S(1)} %pad_clamp_fusion), kind=kCustom, calls=%fused_computation.1 | custom fusion | bytes 2098176 | tf_op jit(solution)/shard_map/gather | solution.py:190
  339.2 3.9 %multiply_reduce_fusion = bf16[64,2048]{1,0:T(8,128)(2,1)} fusion(f32[64,4,2048]{2,1,0:T(4,128)} %reshape.296, f32[64,4]{1,0:T(8,128)S(1)} %copy.106), kind=kLoop, calls=%fused_computation.44 | loop fusion | flops 917504 | bytes 2360320 | tf_op jit(solution)/shard_map/reduce_sum | solution.py:195
  (193 shorter events, 68.1 us)
Async XLA Ops:
  8.0 181.7 %copy-start = (bf16[2,256,2048]{2,1,0:T(8,128)(2,1)S(1)}, bf16[2,256,2048]{2,1,0:T(8,128)(2,1)}, u32[]{:S(2)}) copy-start(bf16[2,256,2048]{2,1,0:T(8,128)(2,1)} %param.31) | copy-start | bytes 6291460
  8.0 228.3 %all-gather.3.cloned.1.call-start = ((), (), s32[]{:S(2)}) async-start(), calls=%async_computation.6 | async-start | bytes 2359296 | tf_op jit(solution)/shard_map/all_gather | solution.py:32
  17.5 109.4 %copy-start.12 = (f32[512]{0:T(512)S(1)}, f32[512]{0:T(512)}, u32[]{:S(2)}) copy-start(f32[512]{0:T(512)} %param.22) | copy-start | bytes 6148
  17.5 109.4 %copy-start.10 = (f32[512,512]{1,0:T(8,128)S(1)}, f32[512,512]{1,0:T(8,128)}, u32[]{:S(2)}) copy-start(f32[512,512]{1,0:T(8,128)} %param.19) | copy-start | bytes 3145732
  74.5 25.5 %collective-permute-start = (bf16[1,8,64,2048]{3,2,1,0:T(8,128)(2,1)S(1)}, bf16[1,8,64,2048]{3,2,1,0:T(8,128)(2,1)S(1)}, u32[]{:S(2)}, u32[]{:S(2)}) collective-permute-start(bf16[1,8,64,2048]{3,2,1,0:T(8,128)(2,1)S(1)} %bitcast.173), channel_id=1, source_target_pairs={{0,1},{1,2},{2,3},{3,0},{4,5},{5,6},{6,7},{7,4},{8,9},{9,10},{10,1... | collective-permute-start | bytes 6291464 | tf_op jit(solution)/shard_map/ppermute | solution.py:19
  100.0 1.3 copy-start.5
  101.3 25.6 %collective-permute-start.1 = (bf16[1,8,64,2048]{3,2,1,0:T(8,128)(2,1)S(1)}, bf16[1,8,64,2048]{3,2,1,0:T(8,128)(2,1)}, u32[]{:S(2)}, u32[]{:S(2)}) collective-permute-start(bf16[1,8,64,2048]{3,2,1,0:T(8,128)(2,1)S(1)} %collective-permute-done), channel_id=1, source_target_pairs={{0,1},{1,2},{2,3},{3,0},{4,5},{5,6},{6,7},{7,4},{8,9},{9,10},{10,1... | collective-permute-start | bytes 6291464 | tf_op jit(solution)/shard_map/ppermute | solution.py:19
  126.9 25.8 %collective-permute-start.2 = (bf16[1,8,64,2048]{3,2,1,0:T(8,128)(2,1)}, bf16[1,8,64,2048]{3,2,1,0:T(8,128)(2,1)}, u32[]{:S(2)}, u32[]{:S(2)}) collective-permute-start(bf16[1,8,64,2048]{3,2,1,0:T(8,128)(2,1)} %collective-permute-done.1), channel_id=1, source_target_pairs={{0,1},{1,2},{2,3},{3,0},{4,5},{5,6},{6,7},{7,4},{8,9},{9,10},{10,1... | collective-permute-start | bytes 6291464 | tf_op jit(solution)/shard_map/ppermute | solution.py:19
  130.2 1.8 copy-start.3
  138.5 140.6 %reduce-scatter.5.cloned.1.call-start = ((), (), s32[]{:S(2)}) async-start(), calls=%async_computation.5 | async-start | bytes 10485760 | tf_op jit(solution)/shard_map/reduce_scatter | solution.py:177
  155.8 3.3 copy-start.6
  159.1 2.3 copy-start.2
  172.2 8.4 %copy-start.15 = (bf16[2,2048,256]{2,1,0:T(8,128)(2,1)S(1)}, bf16[2,2048,256]{2,1,0:T(8,128)(2,1)}, u32[]{:S(2)}) copy-start(bf16[2,2048,256]{2,1,0:T(8,128)(2,1)} %param.29) | copy-start | bytes 6291460
  180.7 5.9 %copy-start.4 = (bf16[4,8,64,2048]{3,2,1,0:T(8,128)(2,1)S(1)}, bf16[4,8,64,2048]{3,2,1,0:T(8,128)(2,1)}, u32[]{:S(2)}) copy-start(bf16[4,8,64,2048]{3,2,1,0:T(8,128)(2,1)} %constant_dynamic-slice_fusion.5) | copy-start | bytes 25165828
  180.7 6.4 %copy-start.16 = (bf16[2,2048,256]{2,1,0:T(8,128)(2,1)S(1)}, bf16[2,2048,256]{2,1,0:T(8,128)(2,1)}, u32[]{:S(2)}) copy-start(bf16[2,2048,256]{2,1,0:T(8,128)(2,1)} %param.30) | copy-start | bytes 6291460
  203.6 139.5 %reduce-scatter.3.cloned.1.call-start = ((), (), s32[]{:S(2)}) async-start(), calls=%async_computation.4 | async-start | bytes 2621440 | tf_op jit(solution)/shard_map/reduce_scatter | solution.py:170
  204.9 2.6 copy-start.9
  204.9 4.0 %copy-start.11 = (bf16[512,512]{1,0:T(8,128)(2,1)S(1)}, bf16[512,512]{1,0:T(8,128)(2,1)}, u32[]{:S(2)}) copy-start(bf16[512,512]{1,0:T(8,128)(2,1)} %param.18) | copy-start | bytes 1572868
  207.6 28.8 %copy-start.14 = (f32[128]{0:T(128)S(1)}, f32[128]{0:T(128)}, u32[]{:S(2)}) copy-start(f32[128]{0:T(128)} %param.23) | copy-start | bytes 1540
  272.9 1.9 copy-start.8
  274.7 1.6 copy-start.17
  274.7 1.7 copy-start.18
  279.1 10.6 %copy-start.13 = (f32[256,4]{0,1:T(4,128)S(1)}, f32[256,4]{0,1:T(4,128)}, u32[]{:S(2)}) copy-start(f32[256,4]{0,1:T(4,128)} %param.28) | copy-start | bytes 12292
  279.2 54.1 %all-to-all-start.1 = ((bf16[8,64,2048]{2,1,0:T(8,128)(2,1)}), bf16[8,64,2048]{2,1,0:T(8,128)(2,1)}, u32[]{:S(2)}, u32[]{:S(2)}) async-start(bf16[8,64,2048]{2,1,0:T(8,128)(2,1)} %bitcast.186), calls=%async_computation.3 | async-start | bytes 4194304 | tf_op jit(solution)/shard_map/all_to_all | solution.py:184
  (2 other events, 2.4 us)
Sparse Core Ops, SparseCore 0:
  138.6 48.4 all-gather.2
Sparse Core Ops, SparseCore 1:
  203.7 70.5 reduce-scatter.4
  279.2 37.1 reduce-scatter.2
